TPU v7x, 32 devices: a whole 2x2x4 slice. The times are simulated.
32 devices in a mesh: sp: 8 (over z, x), tp: 4 (over y, core).
Axes of the slice: x: 2, y: 2, z: 4, core: 2. Of those that a mesh axis runs over, the one named last changes fastest.
Arguments:
- residual: bfloat16 [1024, 2048], P(('sp', 'tp')), may hold values from -6 to 6
- query_first: bfloat16 [1024, 1024], P('sp', 'tp'), may hold values from -200 to 200
- key_first: bfloat16 [1024, 1024], P('sp', 'tp'), may hold values from -200 to 200
- query_second: bfloat16 [1024, 1024], P('sp', 'tp'), may hold values from -200 to 200
- key_second: bfloat16 [1024, 1024], P('sp', 'tp'), may hold values from -200 to 200
- values: bfloat16 [1024, 2048], P('sp', 'tp'), may hold values from -6 to 6
- lambda_weight: float32 [16], P('tp'), may hold values from 0.3 to 0.8
- head_gain: float32 [128], replicated, may hold values from 0.1 to 1.9
- out_weight: bfloat16 [2048, 2048], P('sp', 'tp'), may hold values from -0.125 to 0.125
- norm_gain: float32 [2048], replicated, may hold values from 0.1 to 1.9
- gate_weight: bfloat16 [2048, 5632], P(None, 'tp'), may hold values from -0.125 to 0.125
- up_weight: bfloat16 [2048, 5632], P(None, 'tp'), may hold values from -0.125 to 0.125
- down_weight: bfloat16 [2048, 5632], P('sp', 'tp'), may hold values from -0.078125 to 0.078125
Outputs:
- layer_out: bfloat16 [1024, 2048], P(('sp', 'tp'))
All inputs are finite; a program needn't handle non-finite values.
Results may differ from a plain program's by a relative error of at most 0.017.
Values may be sent and summed in bfloat16 or wider, within the bound.
A program may use at most 128 MiB of HBM per device.

v0:
```python
import functools

import jax
import jax.numpy as jnp
from jax import lax
from jax.experimental import pallas as pl
from jax.experimental.pallas import tpu as pltpu
from jax.sharding import PartitionSpec as P

epsilon = 1e-06
ROWS_ROWS = (((1,), (1,)), ((), ()))
CHUNKS = 4
X_FIRST = 1
PIECES = 2


def split_sp(size):
    inner = 1
    while (2 * inner) * (2 * inner) <= size:
        inner *= 2
    return size // inner, inner


def kernel(
    Z,
    X,
    T,
    C,
    heads,
    residual,
    q_one,
    k_one,
    q_two,
    k_two,
    values,
    lam,
    head_gain,
    out_weight,
    norm_gain,
    gate_weight,
    up_weight,
    down_weight,
    result,
    stage,
    value_stage,
    q_pack,
    k_pack,
    q_all,
    k_all,
    v_all,
    outw,
    downw,
    gate,
    up,
    att_out,
    att,
    res,
    core_out,
    core_in,
    y_out,
    y_in,
    own_sum,
    full,
    normed,
    hidden,
    owner_out,
    owner_in,
    local_sem,
    send_sem,
    recv_sem,
):
    f32, bf16 = jnp.float32, jnp.bfloat16
    scope = jax.named_scope
    s = lax.axis_index("sp")
    t = lax.axis_index("tp")
    z, x = s // X, s % X
    sp = Z * X
    Zh = Z // 2
    G = Zh * X
    half = z // Zh
    other = 1 - half
    zl = z % Zh
    j = zl * X + x
    mate = other * G + j
    Y = T // 2
    y, c = t // 2, t % 2
    tokens = q_one.shape[0]
    piece = tokens // T
    h = s % heads
    first = s - h
    quarter = full.shape[2] // 4

    def z_at(d):
        return (half * Zh + (zl + d) % Zh) * X + x

    def zl_from(d):
        return (zl - d + Zh) % Zh

    def x_at(d):
        return z * X + (x + d) % X

    def x_from(d):
        return (x - d + X) % X

    def t_of(yy, cc):
        return yy * 2 + cc

    def device(sp_at, tp_at):
        return {"sp": sp_at, "tp": tp_at}

    barrier = pltpu.get_barrier_semaphore()
    peers = [((s + d) % sp, t) for d in range(1, sp)]
    peers += [(s, (t + d) % T) for d in range(1, T)]
    peers += [(mate, (t + d) % T) for d in range(1, T)]
    for sp_at, tp_at in peers:
        pl.semaphore_signal(
            barrier, inc=1, device_id=device(sp_at, tp_at), device_id_type=pl.DeviceIdType.MESH
        )

    moves = [
        (k_one, stage.at[0]),
        (k_two, stage.at[1]),
        (q_one, stage.at[2]),
        (q_two, stage.at[3]),
        (values, value_stage),
        (out_weight, outw.at[j]),
        (down_weight, downw.at[j]),
        (gate_weight, gate),
        (up_weight, up),
    ]
    moving = [
        pltpu.make_async_copy(src, dst, local_sem.at[i]) for i, (src, dst) in enumerate(moves)
    ]
    for copy in moving:
        copy.start()

    names = {}
    sends = []

    def slot(name):
        return names.setdefault(name, len(names))

    def send(src, dst, name, sp_at, tp_at):
        k = slot(name)
        pltpu.make_async_remote_copy(
            src_ref=src, dst_ref=dst, send_sem=send_sem.at[k], recv_sem=recv_sem.at[k],
            device_id=device(sp_at, tp_at), device_id_type=pl.DeviceIdType.MESH,
        ).start()

    def wait(ref, name):
        k = slot(name)
        return pltpu.make_async_remote_copy(
            src_ref=ref, dst_ref=ref, send_sem=send_sem.at[k], recv_sem=recv_sem.at[k],
            device_id=device(s, t), device_id_type=pl.DeviceIdType.MESH,
        )

    def arrive(ref, name, same=True):
        wait(ref, name).wait_recv()
        if same:
            sends.append((ref, name))

    with scope("pack"):
        for copy in moving[:4]:
            copy.wait()
        size = stage.shape[2] // heads
        for i in range(heads):
            cols = slice(i * size, (i + 1) * size)
            k_pack[i] = jnp.concatenate([stage[0, :, cols], stage[1, :, cols]], axis=1)
            q_pack[i] = jnp.concatenate([stage[2, :, cols], stage[3, :, cols]], axis=1)
        for copy in moving[4:5]:
            copy.wait()
        value_size = v_all.shape[2]
        k_all[s] = k_pack[h]
        q_all[h] = q_pack[h]
        v_all[s] = value_stage[:, pl.ds(pl.multiple_of(h * value_size, value_size), value_size)]

    with scope("barrier"):
        pl.semaphore_wait(barrier, len(peers))

    targets = [other * G + (j + e) % G for e in range(G)]
    targets += [half * G + (j + e) % G for e in range(1, G)]
    for at in targets:
        send(k_pack.at[at % heads], k_all.at[s], "k", at, t)
    for d in range(1, heads):
        i = (h + d) % heads
        send(q_pack.at[i], q_all.at[h], "q", first + i, t)
    for at in targets:
        start = pl.multiple_of((at % heads) * value_size, value_size)
        send(value_stage.at[:, pl.ds(start, value_size)], v_all.at[s], "v", at, t)

    def out_at(zz, xx):
        return outw.at[zz * X + xx]

    rows_chunk = down_weight.shape[0] // C

    def down_at(k):
        return lambda zz, xx: downw.at[zz * X + xx, pl.ds(k * rows_chunk, rows_chunk)]

    def own_z(name, ref):
        for d in range(1, Zh):
            send(ref(zl, x), ref(zl, x), (name, "z", d), z_at(d), t)

    def own_x(name, ref):
        for d in range(1, X):
            send(ref(zl, x), ref(zl, x), (name, "x", d), x_at(d), t)

    def forward_x(name, ref):
        for d in range(1, Zh):
            block = ref(zl_from(d), x)
            arrive(block, (name, "z", d))
            for dx in range(1, X):
                send(block, block, (name, "zx", d, dx), x_at(dx), t)

    def forward_z(name, ref):
        for d in range(1, X):
            block = ref(zl, x_from(d))
            arrive(block, (name, "x", d))
            for dz in range(1, Zh):
                send(block, block, (name, "xz", d, dz), z_at(dz), t)

    def rest_zx(name, ref):
        for d in range(1, X):
            arrive(ref(zl, x_from(d)), (name, "x", d))
        for d in range(1, Zh):
            for dx in range(1, X):
                arrive(ref(zl_from(d), x_from(dx)), (name, "zx", d, dx))

    def rest_xz(name, ref):
        for d in range(1, Zh):
            arrive(ref(zl_from(d), x), (name, "z", d))
        for d in range(1, X):
            for dz in range(1, Zh):
                arrive(ref(zl_from(dz), x_from(d)), (name, "xz", d, dz))

    z_first = list(range(C - X_FIRST)) if C > X_FIRST else list(range(C))
    x_first = [k for k in range(C) if k not in z_first]

    def down(k):
        return "down%d" % k, down_at(k)

    for copy in moving[5:7]:
        copy.wait()
    own_z("out", out_at)
    own_x("out", out_at)
    for e, sp_at in enumerate((s, mate)):
        side = half if e == 0 else other
        for d in range(2):
            cc = c if d == 0 else 1 - c
            start = pl.multiple_of((side * 2 + cc) * quarter, quarter)
            src = residual.at[:, pl.ds(start, quarter)]
            if e or d:
                send(src, res.at[t], "res", sp_at, t_of(half, cc))
            else:
                k = slot("res")
                k_own = slot("res0")

                @pl.when(y == half)
                def _():
                    pltpu.make_async_copy(src, res.at[t], recv_sem.at[k]).start()

                @pl.when(y != half)
                def _():
                    pltpu.make_async_remote_copy(
                        src_ref=src, dst_ref=res.at[t], send_sem=send_sem.at[k_own],
                        recv_sem=recv_sem.at[k], device_id=device(s, t_of(half, cc)),
                        device_id_type=pl.DeviceIdType.MESH,
                    ).start()
    for k in x_first:
        own_x(*down(k))

    with scope("wait_k"):
        arrive(q_all.at[pl.ds(0, heads - 1)], "q")
        arrive(k_all.at[pl.ds(0, sp - 1)], "k")
    with scope("wait_v"):
        arrive(v_all.at[pl.ds(0, sp - 1)], "v")

    pair = q_all.shape[2]
    head_size = pair // 2
    scale = head_size ** (-0.5)
    block_count = max(1, (sp * tokens) // 1024)
    block_sources = sp // block_count
    block_keys = block_sources * tokens
    lanes = lax.broadcasted_iota(jnp.int32, (1, pair), 1) // head_size

    def maps(q):
        stacked = jnp.concatenate(
            [jnp.where(lanes == i, q, jnp.zeros_like(q)) for i in range(2)], axis=0
        )

        def block(b, state):
            rows = pl.ds(b * block_sources, block_sources)
            scores = lax.dot_general(
                stacked, k_all[rows].reshape(block_keys, pair), ROWS_ROWS,
                preferred_element_type=f32,
            )
            newest = jnp.max(scores, axis=1, keepdims=True)
            if state is not None:
                newest = jnp.maximum(newest, state[0])
            shifted = jnp.exp((scores - newest) * scale)
            totals = jnp.sum(shifted, axis=1, keepdims=True)
            product = jnp.dot(
                shifted.astype(bf16), v_all[rows].reshape(block_keys, value_size),
                preferred_element_type=f32,
            )
            if state is not None:
                factor = jnp.exp((state[0] - newest) * scale)
                totals = totals + state[1] * factor
                product = product + state[2] * factor
            return newest, totals, product

        if block_count == 1:
            state = block(0, None)
        else:
            state = lax.fori_loop(
                0,
                block_count,
                block,
                (
                    jnp.full((2 * tokens, 1), -jnp.inf, f32),
                    jnp.zeros((2 * tokens, 1), f32),
                    jnp.zeros((2 * tokens, value_size), f32),
                ),
            )
        return state[2] / state[1]

    head_cols = pl.ds(pl.multiple_of(h * value_size, value_size), value_size)
    with scope("attention"):
        for d in (*range(1, heads), 0):
            i = (h + d) % heads
            both = maps(q_all[i])
            difference = both[:tokens] - lam[h] * both[tokens:]
            scaled = difference * lax.rsqrt(
                jnp.mean(difference * difference, axis=1, keepdims=True) + epsilon
            )
            att_out[d] = (scaled * head_gain[...]).astype(bf16)
            there = att.at[half, :, head_cols]
            send(att_out.at[d], there, "att_other", other * G + (first + i) % G, t)
            if d:
                send(att_out.at[d], there, "att_own", first + i, t)
            else:
                att[half, :, head_cols] = att_out[d]

    with scope("fwd_out"):
        forward_x("out", out_at)
    for k in z_first[:2]:
        own_z(*down(k))
    with scope("wait_out"):
        rest_zx("out", out_at)
    with scope("wait_att"):
        arrive(v_all.at[pl.ds(0, heads - 1)], "att_own")
        arrive(v_all.at[pl.ds(0, heads)], "att_other")

    core_mate = t_of(y, 1 - c)
    width_out = att.shape[2]
    many = G // 2

    with scope("outproj"):
        rows_in = att[...].reshape(2 * tokens, width_out)

        def project(side):
            weight = outw[pl.ds(side * many, many)].reshape(quarter, width_out)
            return lax.dot_general(rows_in, weight, ROWS_ROWS, preferred_element_type=f32)

        core_out[0] = project(1 - c).astype(bf16)
        send(core_out.at[0], core_in.at[0], "p1c", s, core_mate)
        own_sum[...] = project(c)
        for k in z_first:
            own_x(*down(k))
    with scope("wait_p1c"):
        arrive(core_in.at[0], "p1c")

    def slot_rows(yy):
        return pl.ds(pl.multiple_of(yy * tokens, tokens), tokens)

    with scope("sum_c"):
        for d in range(1, Y):
            yy = (y + d) % Y
            rows = slot_rows(yy)
            y_out[d - 1] = (own_sum[rows] + core_in[0, rows].astype(f32)).astype(bf16)
            send(y_out.at[d - 1], y_in.at[d - 1], ("p1y", d), s, t_of(yy, c))
    with scope("wait_res"):
        wait(res, "res").wait_recv()
    with scope("wait_p1y"):
        for d in range(1, Y):
            arrive(y_in.at[d - 1], ("p1y", d))
    q_own = half * 2 + c
    q_mate = other * 2 + c

    def block_at(yy, q, k=None):
        cols = pl.ds(pl.multiple_of(q * quarter, quarter), quarter)
        size = tokens // PIECES
        rows = pl.ds(0, tokens) if k is None else pl.ds(k * size, size)
        return full.at[yy, rows, cols]

    with scope("sum_y"):
        rows = slot_rows(y)
        total = own_sum[rows] + core_in[0, rows].astype(f32)
        for d in range(1, Y):
            total = total + y_in[d - 1].astype(f32)
        total = total + res[...].reshape(tokens, quarter).astype(f32)
        full[y, :, pl.ds(pl.multiple_of(q_own * quarter, quarter), quarter)] = total.astype(bf16)
        for k in range(PIECES):
            block = block_at(y, q_own, k)
            send(block, block, ("az", k), mate, t)
        for d in range(1, Y):
            block = block_at(y, q_own)
            send(block, block, ("ay", d), s, t_of((y + d) % Y, c))
        block = block_at(y, q_own)
        send(block, block, "ad", s, core_mate)
        for k in z_first[2:] + x_first:
            own_z(*down(k))

    with scope("wait_ay"):
        for d in range(1, Y):
            block = block_at((y - d + Y) % Y, q_own)
            arrive(block, ("ay", d))
            send(block, block, "ad", s, core_mate)
    with scope("wait_az"):
        for k in range(PIECES):
            block = block_at(y, q_mate, k)
            arrive(block, ("az", k))
            for d in range(1, Y):
                send(block, block, ("ayz", d, k), s, t_of((y + d) % Y, c))
            send(block, block, "ad", s, core_mate)
    with scope("fwd_down_a"):
        for k in z_first[:2]:
            forward_x(*down(k))
    with scope("wait_ayz"):
        for k in range(PIECES):
            for d in range(1, Y):
                block = block_at((y - d + Y) % Y, q_mate, k)
                arrive(block, ("ayz", d, k))
                send(block, block, "ad", s, core_mate)
    with scope("wait_ad"):
        arrive(full.at[0], "ad")

    with scope("norm"):
        step = min(32, tokens)
        for yy in range(2):
            for at in range(0, tokens, step):
                stream = full[yy, at : at + step].astype(f32)
                scaled = stream * lax.rsqrt(
                    jnp.mean(stream * stream, axis=1, keepdims=True) + epsilon
                )
                normed[yy * tokens + at : yy * tokens + at + step] = (
                    scaled * norm_gain[...]
                ).astype(bf16)

    for copy in moving[7:]:
        copy.wait()
    width = hidden.shape[1]
    spans = [(at, min(512, width - at)) for at in range(0, width, 512)]
    with scope("gateup"):
        rows_in = normed[...]
        for at, n in spans:
            gate_part = jnp.dot(rows_in, gate[:, at : at + n], preferred_element_type=f32)
            up_part = jnp.dot(rows_in, up[:, at : at + n], preferred_element_type=f32)
            hidden[:, at : at + n] = (
                gate_part / (1.0 + jnp.exp(-gate_part)) * up_part
            ).astype(bf16)
    with scope("fwd_down_b"):
        for k in z_first[2:]:
            forward_x(*down(k))
        for k in x_first:
            forward_z(*down(k))
    with scope("wait_down"):
        for k in z_first:
            rest_zx(*down(k))
        for k in x_first:
            rest_xz(*down(k))

    with scope("downmm"):
        def lower(side):
            weight = downw[pl.ds(side * many, many)].reshape(quarter, width)
            return lax.dot_general(hidden[...], weight, ROWS_ROWS, preferred_element_type=f32)

        core_out[1] = lower(1 - c).astype(bf16)
        send(core_out.at[1], core_in.at[1], "p2c", s, core_mate)
        own_sum[...] = lower(c)
    with scope("wait_p2c"):
        arrive(core_in.at[1], "p2c")
    place = q_own * Y + y
    with scope("sum2"):
        owner_out[...] = (
            (own_sum[...] + core_in[1].astype(f32)).astype(bf16).reshape(2, T, piece, quarter)
        )
        for d in range(T):
            at = (t + d) % T
            send(owner_out.at[other, at], owner_in.at[place], "p2o", mate, at)
        for d in range(1, T):
            at = (t + d) % T
            send(owner_out.at[half, at], owner_in.at[place], "p2o", s, at)
        owner_in[place] = owner_out[half, t]
    with scope("wait_p2o"):
        arrive(owner_in.at[pl.ds(0, 4 * Y - 1)], "p2o")
    with scope("final"):
        mine = pl.ds(pl.multiple_of(t * piece, piece), piece)
        for q in range(4):
            cols = slice(q * quarter, (q + 1) * quarter)
            total = owner_in[q * Y].astype(f32)
            for i in range(1, Y):
                total = total + owner_in[q * Y + i].astype(f32)
            result[:, cols] = (full[half, mine, cols].astype(f32) + total).astype(bf16)
    with scope("wait_send"):
        for ref, name in sends:
            wait(ref, name).wait_send()
        wait(res.at[pl.ds(0, 3)], "res").wait_send()

        @pl.when(y != half)
        def _():
            wait(res.at[0], "res0").wait_send()


def local(Z, X, T, *arrays):
    (residual, q_one, k_one, q_two, k_two, values, lam, head_gain, out_weight, norm_gain,
     gate_weight, up_weight, down_weight) = arrays
    sp = Z * X
    G = sp // 2
    bf16 = jnp.bfloat16
    heads = lam.shape[0]
    tokens, kw = k_one.shape
    vw = values.shape[1]
    pair = 2 * (kw // heads)
    vd = vw // heads
    piece, model = residual.shape
    quarter = model // 4
    width = gate_weight.shape[1]
    rows_down = down_weight.shape[0]
    C = max(1, min(CHUNKS, rows_down // 16))
    Y = T // 2
    vmem = pl.BlockSpec(memory_space=pltpu.VMEM)
    anywhere = pl.BlockSpec(memory_space=pl.ANY)
    smem = pl.BlockSpec(memory_space=pltpu.SMEM)
    Zh = Z // 2
    semaphores = 24 + (1 + C) * (Zh - 1 + X - 1 + (Zh - 1) * (X - 1))
    return pl.pallas_call(
        functools.partial(kernel, Z, X, T, C, heads),
        out_shape=jax.ShapeDtypeStruct((piece, model), bf16),
        in_specs=[
            anywhere, anywhere, anywhere, anywhere, anywhere, anywhere, smem, vmem, anywhere, vmem,
            anywhere, anywhere, anywhere,
        ],
        out_specs=vmem,
        scratch_shapes=[
            pltpu.VMEM((4, tokens, kw), bf16),
            pltpu.VMEM((tokens, vw), bf16),
            pltpu.VMEM((heads, tokens, pair), bf16),
            pltpu.VMEM((heads, tokens, pair), bf16),
            pltpu.VMEM((heads, tokens, pair), bf16),
            pltpu.VMEM((sp, tokens, pair), bf16),
            pltpu.VMEM((sp, tokens, vd), bf16),
            pltpu.VMEM((G, out_weight.shape[0], vw), bf16),
            pltpu.VMEM((G, rows_down, width), bf16),
            pltpu.VMEM(gate_weight.shape, bf16),
            pltpu.VMEM(up_weight.shape, bf16),
            pltpu.VMEM((heads, tokens, vd), bf16),
            pltpu.VMEM((2, tokens, vw), bf16),
            pltpu.VMEM((T, piece, quarter), bf16),
            pltpu.VMEM((2, 2 * tokens, quarter), bf16),
            pltpu.VMEM((2, 2 * tokens, quarter), bf16),
            pltpu.VMEM((Y - 1, tokens, quarter), bf16),
            pltpu.VMEM((Y - 1, tokens, quarter), bf16),
            pltpu.VMEM((2 * tokens, quarter), jnp.float32),
            pltpu.VMEM((2, tokens, model), bf16),
            pltpu.VMEM((2 * tokens, model), bf16),
            pltpu.VMEM((2 * tokens, width), bf16),
            pltpu.VMEM((2, T, piece, quarter), bf16),
            pltpu.VMEM((4 * Y, piece, quarter), bf16),
            pltpu.SemaphoreType.DMA((9,)),
            pltpu.SemaphoreType.DMA((semaphores,)),
            pltpu.SemaphoreType.DMA((semaphores,)),
        ],
        compiler_params=pltpu.CompilerParams(
            collective_id=0, has_side_effects=True, vmem_limit_bytes=60 * 1024 * 1024
        ),
    )(
        residual, q_one, k_one, q_two, k_two, values, lam, head_gain.reshape(1, -1), out_weight,
        norm_gain.reshape(1, -1), gate_weight, up_weight, down_weight,
    )


def solution(mesh):
    Z, X = split_sp(mesh.shape["sp"])
    return jax.shard_map(
        functools.partial(local, Z, X, mesh.shape["tp"]),
        mesh=mesh,
        in_specs=(
            P(("sp", "tp"), None),
            P("sp", "tp"),
            P("sp", "tp"),
            P("sp", "tp"),
            P("sp", "tp"),
            P("sp", "tp"),
            P("tp"),
            P(),
            P("sp", "tp"),
            P(),
            P(None, "tp"),
            P(None, "tp"),
            P("sp", "tp"),
        ),
        out_specs=P(("sp", "tp"), None),
        check_vma=False,
    )
```

profile of v0, /device:TPU:0, one launch (start us, length us, event | category | flops | bytes accessed | tf_op | source)
XLA Modules:
  0.0 74.8 jit_solution(10765012057593271251)
XLA Ops:
  0.0 73.3 %shard_map.127 = bf16[32,2048]{1,0:T(8,128)(2,1)} custom-call(bf16[32,2048]{1,0:T(8,128)(2,1)} %residual.1, bf16[128,256]{1,0:T(8,128)(2,1)} %q_one.1, bf16[128,256]{1,0:T(8,128)(2,1)} %k_one.1, bf16[128,256]{1,0:T(8,128)(2,1)} %q_two.1, bf16[128,256]{1,0:T(8,128)(2,1)} %k_two.1, bf16[128,512]{1,0:T(8,128)(2,1)} %values.1, f32[4]{0:T(128)} %lam.1, ...), custom_call_target="tpu_custom_call" | custom-call | tf_op jit(solution)/shard_map/pallas_call | solution.py:536
  73.3 1.6 %copy.15 = bf16[32,2048]{1,0:T(8,128)(2,1)} copy(bf16[32,2048]{1,0:T(8,128)(2,1)} %shard_map.127) | data formatting | bytes 262144
where the time goes:
time: 75.1 us; the launch traced here: 74.8 us
  Pallas kernels  73.3 us (98%)
  local copies, waits for them, and re-layouts  1.57 us (2%)
    pallas_call x1, Pallas kernels, local(): pl.pallas_call(functools.partial(kernel, Z, X, T, C, heads), out_shape=ja...  73.3 us
    unnamed x1, local copies, waits for them, and re-layouts  1.57 us

commit v1 on v0

--- a/solution.py
+++ b/solution.py
@@ -9,9 +9,13 @@
 
 epsilon = 1e-06
 ROWS_ROWS = (((1,), (1,)), ((), ()))
-CHUNKS = 4
-X_FIRST = 1
-PIECES = 2
+CHUNKS = 8
+X_FIRST = 3
+OUT_CHUNKS = 4
+S0 = 1
+S1 = 1
+S2 = 2
+PIECES = 4
 
 
 def split_sp(size):
@@ -26,6 +30,7 @@
     X,
     T,
     C,
+    OC,
     heads,
     residual,
     q_one,
@@ -57,6 +62,9 @@
     res,
     core_out,
     core_in,
+    prod,
+    lower_out,
+    lower_in,
     y_out,
     y_in,
     own_sum,
@@ -86,6 +94,7 @@
     y, c = t // 2, t % 2
     tokens = q_one.shape[0]
     piece = tokens // T
+    down_rows = down_weight.shape[0]
     h = s % heads
     first = s - h
     quarter = full.shape[2] // 4
@@ -107,6 +116,23 @@
 
     def device(sp_at, tp_at):
         return {"sp": sp_at, "tp": tp_at}
+
+    moves = [
+        (k_one, stage.at[0]),
+        (k_two, stage.at[1]),
+        (q_one, stage.at[2]),
+        (q_two, stage.at[3]),
+        (values, value_stage),
+        (out_weight, outw.at[j]),
+        (down_weight, downw.at[pl.ds(pl.multiple_of(j * down_rows, down_rows), down_rows)]),
+        (gate_weight, gate),
+        (up_weight, up),
+    ]
+    moving = [
+        pltpu.make_async_copy(src, dst, local_sem.at[i]) for i, (src, dst) in enumerate(moves)
+    ]
+    for copy in moving:
+        copy.start()
 
     barrier = pltpu.get_barrier_semaphore()
     peers = [((s + d) % sp, t) for d in range(1, sp)]
@@ -117,47 +143,36 @@
             barrier, inc=1, device_id=device(sp_at, tp_at), device_id_type=pl.DeviceIdType.MESH
         )
 
-    moves = [
-        (k_one, stage.at[0]),
-        (k_two, stage.at[1]),
-        (q_one, stage.at[2]),
-        (q_two, stage.at[3]),
-        (values, value_stage),
-        (out_weight, outw.at[j]),
-        (down_weight, downw.at[j]),
-        (gate_weight, gate),
-        (up_weight, up),
-    ]
-    moving = [
-        pltpu.make_async_copy(src, dst, local_sem.at[i]) for i, (src, dst) in enumerate(moves)
-    ]
-    for copy in moving:
-        copy.start()
-
     names = {}
+    send_names = {}
     sends = []
 
     def slot(name):
         return names.setdefault(name, len(names))
 
-    def send(src, dst, name, sp_at, tp_at):
-        k = slot(name)
+    def send_slot(name):
+        return send_names.setdefault(name, len(send_names))
+
+    def send(src, dst, name, sp_at, tp_at, group=None):
         pltpu.make_async_remote_copy(
-            src_ref=src, dst_ref=dst, send_sem=send_sem.at[k], recv_sem=recv_sem.at[k],
-            device_id=device(sp_at, tp_at), device_id_type=pl.DeviceIdType.MESH,
+            src_ref=src, dst_ref=dst, send_sem=send_sem.at[send_slot(group or name)],
+            recv_sem=recv_sem.at[slot(name)], device_id=device(sp_at, tp_at),
+            device_id_type=pl.DeviceIdType.MESH,
         ).start()
 
-    def wait(ref, name):
-        k = slot(name)
+    def wait(ref, send_at, recv_at):
         return pltpu.make_async_remote_copy(
-            src_ref=ref, dst_ref=ref, send_sem=send_sem.at[k], recv_sem=recv_sem.at[k],
+            src_ref=ref, dst_ref=ref, send_sem=send_sem.at[send_at], recv_sem=recv_sem.at[recv_at],
             device_id=device(s, t), device_id_type=pl.DeviceIdType.MESH,
         )
 
     def arrive(ref, name, same=True):
-        wait(ref, name).wait_recv()
+        wait(ref, 0, slot(name)).wait_recv()
         if same:
             sends.append((ref, name))
+
+    def sent(ref, name):
+        wait(ref, send_slot(name), 0).wait_send()
 
     with scope("pack"):
         for copy in moving[:4]:
@@ -188,60 +203,58 @@
         start = pl.multiple_of((at % heads) * value_size, value_size)
         send(value_stage.at[:, pl.ds(start, value_size)], v_all.at[s], "v", at, t)
 
-    def out_at(zz, xx):
-        return outw.at[zz * X + xx]
-
-    rows_chunk = down_weight.shape[0] // C
-
-    def down_at(k):
-        return lambda zz, xx: downw.at[zz * X + xx, pl.ds(k * rows_chunk, rows_chunk)]
-
-    def own_z(name, ref):
+    def rows_of(ref, count, k):
+        size = ref.shape[1] // count
+        return lambda zz, xx: ref.at[zz * X + xx, pl.ds(k * size, size)]
+
+    def down_part(k):
+        size = down_rows // C
+
+        def at(zz, xx):
+            start = pl.multiple_of((zz * X + xx) * down_rows + k * size, size)
+            return downw.at[pl.ds(start, size)]
+
+        return at
+
+    def own_z(name, ref, group, last):
         for d in range(1, Zh):
-            send(ref(zl, x), ref(zl, x), (name, "z", d), z_at(d), t)
-
-    def own_x(name, ref):
+            to = group + "_z" if last else (name, "z", d)
+            send(ref(zl, x), ref(zl, x), to, z_at(d), t, group)
+
+    def own_x(name, ref, group, last):
         for d in range(1, X):
-            send(ref(zl, x), ref(zl, x), (name, "x", d), x_at(d), t)
-
-    def forward_x(name, ref):
+            to = group + "_x" if last else (name, "x", d)
+            send(ref(zl, x), ref(zl, x), to, x_at(d), t, group)
+
+    def forward_x(name, ref, group):
         for d in range(1, Zh):
             block = ref(zl_from(d), x)
-            arrive(block, (name, "z", d))
+            arrive(block, (name, "z", d), False)
             for dx in range(1, X):
-                send(block, block, (name, "zx", d, dx), x_at(dx), t)
-
-    def forward_z(name, ref):
+                send(block, block, group + "_rest", x_at(dx), t, group)
+
+    def forward_z(name, ref, group):
         for d in range(1, X):
             block = ref(zl, x_from(d))
-            arrive(block, (name, "x", d))
+            arrive(block, (name, "x", d), False)
             for dz in range(1, Zh):
-                send(block, block, (name, "xz", d, dz), z_at(dz), t)
-
-    def rest_zx(name, ref):
-        for d in range(1, X):
-            arrive(ref(zl, x_from(d)), (name, "x", d))
-        for d in range(1, Zh):
-            for dx in range(1, X):
-                arrive(ref(zl_from(d), x_from(dx)), (name, "zx", d, dx))
-
-    def rest_xz(name, ref):
-        for d in range(1, Zh):
-            arrive(ref(zl_from(d), x), (name, "z", d))
-        for d in range(1, X):
-            for dz in range(1, Zh):
-                arrive(ref(zl_from(dz), x_from(d)), (name, "xz", d, dz))
+                send(block, block, group + "_rest", z_at(dz), t, group)
+
+    def down(k):
+        return "down%d" % k, down_part(k), "down"
+
+    def out(k):
+        return "out%d" % k, rows_of(outw, OC, k), "out"
 
     z_first = list(range(C - X_FIRST)) if C > X_FIRST else list(range(C))
     x_first = [k for k in range(C) if k not in z_first]
 
-    def down(k):
-        return "down%d" % k, down_at(k)
-
+    nx = len(x_first)
     for copy in moving[5:7]:
         copy.wait()
-    own_z("out", out_at)
-    own_x("out", out_at)
+    for k in range(OC):
+        own_z(*out(k), False)
+        own_x(*out(k), True)
     for e, sp_at in enumerate((s, mate)):
         side = half if e == 0 else other
         for d in range(2):
@@ -252,7 +265,7 @@
                 send(src, res.at[t], "res", sp_at, t_of(half, cc))
             else:
                 k = slot("res")
-                k_own = slot("res0")
+                k_own = send_slot("res0")
 
                 @pl.when(y == half)
                 def _():
@@ -265,8 +278,8 @@
                         recv_sem=recv_sem.at[k], device_id=device(s, t_of(half, cc)),
                         device_id_type=pl.DeviceIdType.MESH,
                     ).start()
-    for k in x_first:
-        own_x(*down(k))
+    for k in x_first[:S0]:
+        own_x(*down(k), False)
 
     with scope("wait_k"):
         arrive(q_all.at[pl.ds(0, heads - 1)], "q")
@@ -325,7 +338,7 @@
 
     head_cols = pl.ds(pl.multiple_of(h * value_size, value_size), value_size)
     with scope("attention"):
-        for d in (*range(1, heads), 0):
+        for turn, d in enumerate((*range(1, heads), 0)):
             i = (h + d) % heads
             both = maps(q_all[i])
             difference = both[:tokens] - lam[h] * both[tokens:]
@@ -339,16 +352,27 @@
                 send(att_out.at[d], there, "att_own", first + i, t)
             else:
                 att[half, :, head_cols] = att_out[d]
+            if 0 < turn <= OC:
+                forward_x(*out(turn - 1))
 
     with scope("fwd_out"):
-        forward_x("out", out_at)
-    for k in z_first[:2]:
-        own_z(*down(k))
+        for k in range(heads - 1, OC):
+            forward_x(*out(k))
+        for k in x_first[S0 : S0 + S1]:
+            own_x(*down(k), False)
+        for k in z_first[:S2]:
+            own_z(*down(k), False)
+    with scope("wait_att_own"):
+        arrive(v_all.at[pl.ds(0, heads - 1)], "att_own")
+    with scope("wait_att"):
+        arrive(v_all.at[pl.ds(0, heads)], "att_other")
     with scope("wait_out"):
-        rest_zx("out", out_at)
-    with scope("wait_att"):
-        arrive(v_all.at[pl.ds(0, heads - 1)], "att_own")
-        arrive(v_all.at[pl.ds(0, heads)], "att_other")
+        arrive(outw.at[pl.ds(0, X - 1)], "out_x", False)
+        arrive(outw.at[pl.ds(0, (X - 1) * (Zh - 1))], "out_rest", False)
+    for k in z_first[S2:]:
+        own_z(*down(k), False)
+    for k in x_first[S0 + S1 :]:
+        own_x(*down(k), False)
 
     core_mate = t_of(y, 1 - c)
     width_out = att.shape[2]
@@ -365,71 +389,87 @@
         send(core_out.at[0], core_in.at[0], "p1c", s, core_mate)
         own_sum[...] = project(c)
         for k in z_first:
-            own_x(*down(k))
+            own_x(*down(k), True)
     with scope("wait_p1c"):
         arrive(core_in.at[0], "p1c")
 
     def slot_rows(yy):
         return pl.ds(pl.multiple_of(yy * tokens, tokens), tokens)
 
+    part = tokens // PIECES
+
+    def slot_rows(yy, k):
+        return pl.ds(pl.multiple_of(yy * tokens + k * part, part), part)
+
     with scope("sum_c"):
-        for d in range(1, Y):
-            yy = (y + d) % Y
-            rows = slot_rows(yy)
-            y_out[d - 1] = (own_sum[rows] + core_in[0, rows].astype(f32)).astype(bf16)
-            send(y_out.at[d - 1], y_in.at[d - 1], ("p1y", d), s, t_of(yy, c))
+        for k in range(PIECES):
+            for d in range(1, Y):
+                yy = (y + d) % Y
+                rows = slot_rows(yy, k)
+                block = y_out.at[d - 1, pl.ds(k * part, part)]
+                y_out[d - 1, k * part : (k + 1) * part] = (
+                    own_sum[rows] + core_in[0, rows].astype(f32)
+                ).astype(bf16)
+                there = y_in.at[d - 1, pl.ds(k * part, part)]
+                send(block, there, ("p1y", d, k), s, t_of(yy, c), "after")
     with scope("wait_res"):
-        wait(res, "res").wait_recv()
-    with scope("wait_p1y"):
-        for d in range(1, Y):
-            arrive(y_in.at[d - 1], ("p1y", d))
+        arrive(res, "res", False)
     q_own = half * 2 + c
     q_mate = other * 2 + c
 
     def block_at(yy, q, k=None):
         cols = pl.ds(pl.multiple_of(q * quarter, quarter), quarter)
-        size = tokens // PIECES
-        rows = pl.ds(0, tokens) if k is None else pl.ds(k * size, size)
+        rows = pl.ds(0, tokens) if k is None else pl.ds(k * part, part)
         return full.at[yy, rows, cols]
 
     with scope("sum_y"):
-        rows = slot_rows(y)
-        total = own_sum[rows] + core_in[0, rows].astype(f32)
-        for d in range(1, Y):
-            total = total + y_in[d - 1].astype(f32)
-        total = total + res[...].reshape(tokens, quarter).astype(f32)
-        full[y, :, pl.ds(pl.multiple_of(q_own * quarter, quarter), quarter)] = total.astype(bf16)
+        residual_rows = res[...].reshape(tokens, quarter)
+        own_cols = pl.ds(pl.multiple_of(q_own * quarter, quarter), quarter)
         for k in range(PIECES):
+            rows = slot_rows(y, k)
+            here = slice(k * part, (k + 1) * part)
+            total = own_sum[rows] + core_in[0, rows].astype(f32)
+            for d in range(1, Y):
+                arrive(y_in.at[d - 1, pl.ds(k * part, part)], ("p1y", d, k), False)
+                total = total + y_in[d - 1, here].astype(f32)
+            total = total + residual_rows[here].astype(f32)
+            full[y, here, own_cols] = total.astype(bf16)
             block = block_at(y, q_own, k)
-            send(block, block, ("az", k), mate, t)
-        for d in range(1, Y):
-            block = block_at(y, q_own)
-            send(block, block, ("ay", d), s, t_of((y + d) % Y, c))
+            send(block, block, ("az", k), mate, t, "after")
+            for d in range(1, Y):
+                send(block, block, ("ay", d), s, t_of((y + d) % Y, c), "after")
         block = block_at(y, q_own)
         send(block, block, "ad", s, core_mate)
-        for k in z_first[2:] + x_first:
-            own_z(*down(k))
+    with scope("bulk_a"):
+        for k in z_first[:3]:
+            forward_x(*down(k))
+        for k in x_first[: nx - 1]:
+            own_z(*down(k), True)
+            forward_z(*down(k))
 
     with scope("wait_ay"):
         for d in range(1, Y):
             block = block_at((y - d + Y) % Y, q_own)
-            arrive(block, ("ay", d))
+            arrive(block, ("ay", d), False)
             send(block, block, "ad", s, core_mate)
     with scope("wait_az"):
         for k in range(PIECES):
             block = block_at(y, q_mate, k)
-            arrive(block, ("az", k))
+            arrive(block, ("az", k), False)
             for d in range(1, Y):
-                send(block, block, ("ayz", d, k), s, t_of((y + d) % Y, c))
+                send(block, block, ("ayz", d, k), s, t_of((y + d) % Y, c), "after")
             send(block, block, "ad", s, core_mate)
-    with scope("fwd_down_a"):
-        for k in z_first[:2]:
+    with scope("bulk_b"):
+        for k in z_first[3:]:
             forward_x(*down(k))
+        for k in x_first[nx - 1 :]:
+            own_z(*down(k), True)
+            forward_z(*down(k))
     with scope("wait_ayz"):
         for k in range(PIECES):
             for d in range(1, Y):
                 block = block_at((y - d + Y) % Y, q_mate, k)
-                arrive(block, ("ayz", d, k))
+                arrive(block, ("ayz", d, k), False)
                 send(block, block, "ad", s, core_mate)
     with scope("wait_ad"):
         arrive(full.at[0], "ad")
@@ -458,57 +498,106 @@
             hidden[:, at : at + n] = (
                 gate_part / (1.0 + jnp.exp(-gate_part)) * up_part
             ).astype(bf16)
-    with scope("fwd_down_b"):
-        for k in z_first[2:]:
-            forward_x(*down(k))
-        for k in x_first:
-            forward_z(*down(k))
-    with scope("wait_down"):
-        for k in z_first:
-            rest_zx(*down(k))
-        for k in x_first:
-            rest_xz(*down(k))
-
-    with scope("downmm"):
-        def lower(side):
-            weight = downw[pl.ds(side * many, many)].reshape(quarter, width)
-            return lax.dot_general(hidden[...], weight, ROWS_ROWS, preferred_element_type=f32)
-
-        core_out[1] = lower(1 - c).astype(bf16)
-        send(core_out.at[1], core_in.at[1], "p2c", s, core_mate)
-        own_sum[...] = lower(c)
-    with scope("wait_p2c"):
-        arrive(core_in.at[1], "p2c")
     place = q_own * Y + y
-    with scope("sum2"):
-        owner_out[...] = (
-            (own_sum[...] + core_in[1].astype(f32)).astype(bf16).reshape(2, T, piece, quarter)
-        )
+    unit = prod.shape[2]
+    half_unit = unit // 2
+    size = down_rows // C
+    staged = G == 4 and X == 2
+    if staged:
+        order = [j, zl * X + 1 - x, (1 - zl) * X + x, (1 - zl) * X + 1 - x]
+    else:
+        order = list(range(4))
+
+    def lower(i):
+        weight = downw[pl.ds(pl.multiple_of(order[i] * unit, unit), unit)]
+        prod[i] = lax.dot_general(hidden[...], weight, ROWS_ROWS, preferred_element_type=f32)
+        cols = pl.ds(pl.multiple_of((1 - c) * half_unit, half_unit), half_unit)
+        lower_out[i] = prod[i, :, cols].astype(bf16)
+
+    def pass_on(lo, n, name):
+        units = pl.ds(lo, n)
+        send(lower_out.at[units], lower_in.at[units], name, s, core_mate)
+
+    def to_owners(lo, n, name, core_name):
+        units = pl.ds(lo, n)
+        arrive(lower_in.at[units], core_name)
+        cols = pl.ds(pl.multiple_of(c * half_unit, half_unit), half_unit)
+        for i in range(lo, lo + n):
+            total = prod[i, :, cols] + lower_in[i].astype(f32)
+            owner_out[:, :, i] = total.astype(bf16).reshape(2, T, piece, half_unit)
         for d in range(T):
             at = (t + d) % T
-            send(owner_out.at[other, at], owner_in.at[place], "p2o", mate, at)
+            send(owner_out.at[other, at, units], owner_in.at[place, units], name, mate, at)
         for d in range(1, T):
             at = (t + d) % T
-            send(owner_out.at[half, at], owner_in.at[place], "p2o", s, at)
-        owner_in[place] = owner_out[half, t]
+            send(owner_out.at[half, at, units], owner_in.at[place, units], name, s, at)
+        owner_in[place, units] = owner_out[half, t, units]
+
+    def wait_x():
+        if z_first:
+            arrive(downw.at[pl.ds(0, len(z_first) * (X - 1) * size)], "down_x", False)
+
+    def wait_z():
+        if x_first:
+            arrive(downw.at[pl.ds(0, nx * (Zh - 1) * size)], "down_z", False)
+
+    def wait_rest():
+        arrive(downw.at[pl.ds(0, (X - 1) * (Zh - 1) * down_rows)], "down_rest", False)
+
+    if not staged:
+        wait_x()
+        wait_z()
+        wait_rest()
+    with scope("down_a"):
+        lower(0)
+        if staged:
+            with scope("wait_x"):
+                wait_x()
+        lower(1)
+        if staged:
+            with scope("wait_z"):
+                wait_z()
+        lower(2)
+        pass_on(0, 3, "p2c")
+    with scope("owners_a"):
+        to_owners(0, 3, "p2o", "p2c")
+    if staged:
+        with scope("wait_rest"):
+            wait_rest()
+    with scope("down_b"):
+        lower(3)
+        pass_on(3, 1, "p3c")
+        to_owners(3, 1, "p3o", "p3c")
+    mine = pl.ds(pl.multiple_of(t * piece, piece), piece)
+
+    def finish(lo, n, name):
+        arrive(owner_in.at[pl.ds(0, 4 * Y - 1), pl.ds(lo, n)], name)
+        for q in range(4):
+            for i in range(lo, lo + n):
+                start = (q // 2) * 4 * unit + order[i] * unit + (q % 2) * half_unit
+                cols = pl.ds(pl.multiple_of(start, half_unit), half_unit)
+                total = owner_in[q * Y, i].astype(f32)
+                for k in range(1, Y):
+                    total = total + owner_in[q * Y + k, i].astype(f32)
+                result[:, cols] = (full[half, mine, cols].astype(f32) + total).astype(bf16)
+
     with scope("wait_p2o"):
-        arrive(owner_in.at[pl.ds(0, 4 * Y - 1)], "p2o")
-    with scope("final"):
-        mine = pl.ds(pl.multiple_of(t * piece, piece), piece)
-        for q in range(4):
-            cols = slice(q * quarter, (q + 1) * quarter)
-            total = owner_in[q * Y].astype(f32)
-            for i in range(1, Y):
-                total = total + owner_in[q * Y + i].astype(f32)
-            result[:, cols] = (full[half, mine, cols].astype(f32) + total).astype(bf16)
+        finish(0, 3, "p2o")
+    with scope("wait_p3o"):
+        finish(3, 1, "p3o")
     with scope("wait_send"):
         for ref, name in sends:
-            wait(ref, name).wait_send()
-        wait(res.at[pl.ds(0, 3)], "res").wait_send()
+            sent(ref, name)
+        sent(outw.at[pl.ds(0, G - 1)], "out")
+        sent(downw.at[pl.ds(0, (G - 1) * down_rows)], "down")
+        assert 3 * (Y - 1) + 1 == 4
+        sent(full.at[0], "after")
+        sent(res.at[pl.ds(0, 3)], "res")
 
         @pl.when(y != half)
         def _():
-            wait(res.at[0], "res0").wait_send()
+            sent(res.at[0], "res0")
+    assert len(names) <= recv_sem.shape[0] and len(send_names) <= send_sem.shape[0]
 
 
 def local(Z, X, T, *arrays):
@@ -527,14 +616,16 @@
     width = gate_weight.shape[1]
     rows_down = down_weight.shape[0]
     C = max(1, min(CHUNKS, rows_down // 16))
+    OC = max(1, min(OUT_CHUNKS, out_weight.shape[0] // 16))
     Y = T // 2
     vmem = pl.BlockSpec(memory_space=pltpu.VMEM)
     anywhere = pl.BlockSpec(memory_space=pl.ANY)
     smem = pl.BlockSpec(memory_space=pltpu.SMEM)
     Zh = Z // 2
-    semaphores = 24 + (1 + C) * (Zh - 1 + X - 1 + (Zh - 1) * (X - 1))
+    z_first = C - X_FIRST if C > X_FIRST else C
+    received = 20 + 4 * PIECES + (OC + z_first) * (Zh - 1) + (C - z_first) * (X - 1)
     return pl.pallas_call(
-        functools.partial(kernel, Z, X, T, C, heads),
+        functools.partial(kernel, Z, X, T, C, OC, heads),
         out_shape=jax.ShapeDtypeStruct((piece, model), bf16),
         in_specs=[
             anywhere, anywhere, anywhere, anywhere, anywhere, anywhere, smem, vmem, anywhere, vmem,
@@ -550,25 +641,28 @@
             pltpu.VMEM((sp, tokens, pair), bf16),
             pltpu.VMEM((sp, tokens, vd), bf16),
             pltpu.VMEM((G, out_weight.shape[0], vw), bf16),
-            pltpu.VMEM((G, rows_down, width), bf16),
+            pltpu.VMEM((G * rows_down, width), bf16),
             pltpu.VMEM(gate_weight.shape, bf16),
             pltpu.VMEM(up_weight.shape, bf16),
             pltpu.VMEM((heads, tokens, vd), bf16),
             pltpu.VMEM((2, tokens, vw), bf16),
             pltpu.VMEM((T, piece, quarter), bf16),
-            pltpu.VMEM((2, 2 * tokens, quarter), bf16),
-            pltpu.VMEM((2, 2 * tokens, quarter), bf16),
+            pltpu.VMEM((1, 2 * tokens, quarter), bf16),
+            pltpu.VMEM((1, 2 * tokens, quarter), bf16),
+            pltpu.VMEM((4, 2 * tokens, model // 8), jnp.float32),
+            pltpu.VMEM((4, 2 * tokens, model // 16), bf16),
+            pltpu.VMEM((4, 2 * tokens, model // 16), bf16),
             pltpu.VMEM((Y - 1, tokens, quarter), bf16),
             pltpu.VMEM((Y - 1, tokens, quarter), bf16),
             pltpu.VMEM((2 * tokens, quarter), jnp.float32),
             pltpu.VMEM((2, tokens, model), bf16),
             pltpu.VMEM((2 * tokens, model), bf16),
             pltpu.VMEM((2 * tokens, width), bf16),
-            pltpu.VMEM((2, T, piece, quarter), bf16),
-            pltpu.VMEM((4 * Y, piece, quarter), bf16),
+            pltpu.VMEM((2, T, 4, piece, model // 16), bf16),
+            pltpu.VMEM((4 * Y, 4, piece, model // 16), bf16),
             pltpu.SemaphoreType.DMA((9,)),
-            pltpu.SemaphoreType.DMA((semaphores,)),
-            pltpu.SemaphoreType.DMA((semaphores,)),
+            pltpu.SemaphoreType.DMA((16,)),
+            pltpu.SemaphoreType.DMA((received,)),
         ],
         compiler_params=pltpu.CompilerParams(
             collective_id=0, has_side_effects=True, vmem_limit_bytes=60 * 1024 * 1024

time: 75.1 us -> 64.8 us (0.86)
  Pallas kernels: 73.3 us -> 63 us
    pallas_call x1, Pallas kernels: 73.3 us -> 63 us  [local(): pl.pallas_call(functools.partial(kernel, Z, X, T, C, OC, heads), out_shap...]
where the time goes in v1:
time: 64.8 us; the launch traced here: 64.6 us
  Pallas kernels  63 us (97%)
  local copies, waits for them, and re-layouts  1.57 us (2%)
    pallas_call x1, Pallas kernels, local(): pl.pallas_call(functools.partial(kernel, Z, X, T, C, OC, heads), out_shap...  63 us
    unnamed x1, local copies, waits for them, and re-layouts  1.57 us

profile of v1, /device:TPU:0, one launch (start us, length us, event | category | flops | bytes accessed | tf_op | source)
XLA Modules:
  0.0 64.6 jit_solution(944466977983364234)
XLA Ops:
  0.0 63.0 %shard_map.127 = bf16[32,2048]{1,0:T(8,128)(2,1)} custom-call(bf16[32,2048]{1,0:T(8,128)(2,1)} %residual.1, bf16[128,256]{1,0:T(8,128)(2,1)} %q_one.1, bf16[128,256]{1,0:T(8,128)(2,1)} %k_one.1, bf16[128,256]{1,0:T(8,128)(2,1)} %q_two.1, bf16[128,256]{1,0:T(8,128)(2,1)} %k_two.1, bf16[128,512]{1,0:T(8,128)(2,1)} %values.1, f32[4]{0:T(128)} %lam.1, ...), custom_call_target="tpu_custom_call" | custom-call | tf_op jit(solution)/shard_map/pallas_call | solution.py:627
  63.0 1.6 %copy.15 = bf16[32,2048]{1,0:T(8,128)(2,1)} copy(bf16[32,2048]{1,0:T(8,128)(2,1)} %shard_map.127) | data formatting | bytes 262144

commit v2 on v1

--- a/solution.py
+++ b/solution.py
@@ -10,11 +10,13 @@
 epsilon = 1e-06
 ROWS_ROWS = (((1,), (1,)), ((), ()))
 CHUNKS = 8
+S3 = 1
 X_FIRST = 3
 OUT_CHUNKS = 4
 S0 = 1
 S1 = 1
-S2 = 2
+S2 = 5
+OUT_X_FIRST = 0
 PIECES = 4
 
 
@@ -57,6 +59,10 @@
     downw,
     gate,
     up,
+    head_scale,
+    norm_scale,
+    rounded_all,
+    totals_all,
     att_out,
     att,
     res,
@@ -70,6 +76,10 @@
     own_sum,
     full,
     normed,
+    squares,
+    inverse,
+    gate_sum,
+    up_sum,
     hidden,
     owner_out,
     owner_in,
@@ -127,6 +137,8 @@
         (down_weight, downw.at[pl.ds(pl.multiple_of(j * down_rows, down_rows), down_rows)]),
         (gate_weight, gate),
         (up_weight, up),
+        (head_gain, head_scale),
+        (norm_gain, norm_scale),
     ]
     moving = [
         pltpu.make_async_copy(src, dst, local_sem.at[i]) for i, (src, dst) in enumerate(moves)
@@ -252,9 +264,11 @@
     nx = len(x_first)
     for copy in moving[5:7]:
         copy.wait()
+    out_z_first = list(range(OC - OUT_X_FIRST)) if OC > OUT_X_FIRST else list(range(OC))
+    out_x_first = [k for k in range(OC) if k not in out_z_first]
     for k in range(OC):
-        own_z(*out(k), False)
-        own_x(*out(k), True)
+        own_z(*out(k), k in out_x_first)
+        own_x(*out(k), k in out_z_first)
     for e, sp_at in enumerate((s, mate)):
         side = half if e == 0 else other
         for d in range(2):
@@ -284,9 +298,6 @@
     with scope("wait_k"):
         arrive(q_all.at[pl.ds(0, heads - 1)], "q")
         arrive(k_all.at[pl.ds(0, sp - 1)], "k")
-    with scope("wait_v"):
-        arrive(v_all.at[pl.ds(0, sp - 1)], "v")
-
     pair = q_all.shape[2]
     head_size = pair // 2
     scale = head_size ** (-0.5)
@@ -295,10 +306,13 @@
     block_keys = block_sources * tokens
     lanes = lax.broadcasted_iota(jnp.int32, (1, pair), 1) // head_size
 
-    def maps(q):
-        stacked = jnp.concatenate(
+    def stack(q):
+        return jnp.concatenate(
             [jnp.where(lanes == i, q, jnp.zeros_like(q)) for i in range(2)], axis=0
         )
+
+    def maps(q):
+        stacked = stack(q)
 
         def block(b, state):
             rows = pl.ds(b * block_sources, block_sources)
@@ -307,70 +321,96 @@
                 preferred_element_type=f32,
             )
             newest = jnp.max(scores, axis=1, keepdims=True)
-            if state is not None:
-                newest = jnp.maximum(newest, state[0])
+            newest = jnp.maximum(newest, state[0])
             shifted = jnp.exp((scores - newest) * scale)
             totals = jnp.sum(shifted, axis=1, keepdims=True)
             product = jnp.dot(
                 shifted.astype(bf16), v_all[rows].reshape(block_keys, value_size),
                 preferred_element_type=f32,
             )
-            if state is not None:
-                factor = jnp.exp((state[0] - newest) * scale)
-                totals = totals + state[1] * factor
-                product = product + state[2] * factor
+            factor = jnp.exp((state[0] - newest) * scale)
+            totals = totals + state[1] * factor
+            product = product + state[2] * factor
             return newest, totals, product
 
-        if block_count == 1:
-            state = block(0, None)
+        state = lax.fori_loop(
+            0,
+            block_count,
+            block,
+            (
+                jnp.full((2 * tokens, 1), -jnp.inf, f32),
+                jnp.zeros((2 * tokens, 1), f32),
+                jnp.zeros((2 * tokens, value_size), f32),
+            ),
+        )
+        return state[2] / state[1]
+
+    moving[9].wait()
+    head_cols = pl.ds(pl.multiple_of(h * value_size, value_size), value_size)
+    turns = (*range(1, heads), 0)
+
+    def attend(d, both):
+        difference = both[:tokens] - lam[h] * both[tokens:]
+        scaled = difference * lax.rsqrt(
+            jnp.mean(difference * difference, axis=1, keepdims=True) + epsilon
+        )
+        att_out[d] = (scaled * head_scale[...]).astype(bf16)
+        there = att.at[half, :, head_cols]
+        i = (h + d) % heads
+        send(att_out.at[d], there, "att_other", other * G + (first + i) % G, t)
+        if d:
+            send(att_out.at[d], there, "att_own", first + i, t)
         else:
-            state = lax.fori_loop(
-                0,
-                block_count,
-                block,
-                (
-                    jnp.full((2 * tokens, 1), -jnp.inf, f32),
-                    jnp.zeros((2 * tokens, 1), f32),
-                    jnp.zeros((2 * tokens, value_size), f32),
-                ),
-            )
-        return state[2] / state[1]
-
-    head_cols = pl.ds(pl.multiple_of(h * value_size, value_size), value_size)
-    with scope("attention"):
-        for turn, d in enumerate((*range(1, heads), 0)):
-            i = (h + d) % heads
-            both = maps(q_all[i])
-            difference = both[:tokens] - lam[h] * both[tokens:]
-            scaled = difference * lax.rsqrt(
-                jnp.mean(difference * difference, axis=1, keepdims=True) + epsilon
-            )
-            att_out[d] = (scaled * head_gain[...]).astype(bf16)
-            there = att.at[half, :, head_cols]
-            send(att_out.at[d], there, "att_other", other * G + (first + i) % G, t)
-            if d:
-                send(att_out.at[d], there, "att_own", first + i, t)
-            else:
-                att[half, :, head_cols] = att_out[d]
-            if 0 < turn <= OC:
-                forward_x(*out(turn - 1))
+            att[half, :, head_cols] = att_out[d]
+
+    if block_count == 1:
+        with scope("scores"):
+            for d in turns:
+                scores = lax.dot_general(
+                    stack(q_all[(h + d) % heads]), k_all[...].reshape(block_keys, pair), ROWS_ROWS,
+                    preferred_element_type=f32,
+                )
+                newest = jnp.max(scores, axis=1, keepdims=True)
+                shifted = jnp.exp((scores - newest) * scale)
+                totals_all[d] = jnp.sum(shifted, axis=1, keepdims=True)
+                rounded_all[d] = shifted.astype(bf16)
+        with scope("wait_v"):
+            arrive(v_all.at[pl.ds(0, sp - 1)], "v")
+        with scope("attention"):
+            for d in turns:
+                product = jnp.dot(
+                    rounded_all[d], v_all[...].reshape(block_keys, value_size),
+                    preferred_element_type=f32,
+                )
+                attend(d, product / totals_all[d])
+    else:
+        arrive(v_all.at[pl.ds(0, sp - 1)], "v")
+        for d in turns:
+            attend(d, maps(q_all[(h + d) % heads]))
 
     with scope("fwd_out"):
-        for k in range(heads - 1, OC):
+        for k in out_x_first:
+            forward_z(*out(k))
+        for k in out_z_first:
             forward_x(*out(k))
-        for k in x_first[S0 : S0 + S1]:
-            own_x(*down(k), False)
         for k in z_first[:S2]:
             own_z(*down(k), False)
     with scope("wait_att_own"):
         arrive(v_all.at[pl.ds(0, heads - 1)], "att_own")
     with scope("wait_att"):
+        for k in x_first[S0 : S0 + S1]:
+            own_x(*down(k), False)
         arrive(v_all.at[pl.ds(0, heads)], "att_other")
     with scope("wait_out"):
-        arrive(outw.at[pl.ds(0, X - 1)], "out_x", False)
+        size_out = outw.shape[1] // OC
+        arrive(outw.at[pl.ds(0, X - 1), pl.ds(0, len(out_z_first) * size_out)], "out_x", False)
+        if out_x_first:
+            arrive(outw.at[pl.ds(0, Zh - 1), pl.ds(0, len(out_x_first) * size_out)], "out_z", False)
         arrive(outw.at[pl.ds(0, (X - 1) * (Zh - 1))], "out_rest", False)
     for k in z_first[S2:]:
         own_z(*down(k), False)
+    for k in x_first[:S3]:
+        own_z(*down(k), True)
     for k in x_first[S0 + S1 :]:
         own_x(*down(k), False)
 
@@ -386,12 +426,19 @@
             return lax.dot_general(rows_in, weight, ROWS_ROWS, preferred_element_type=f32)
 
         core_out[0] = project(1 - c).astype(bf16)
-        send(core_out.at[0], core_in.at[0], "p1c", s, core_mate)
+        for d in (*range(1, Y), 0):
+            lines = pl.ds(pl.multiple_of((y + d) % Y * tokens, tokens), tokens)
+            send(core_out.at[0, lines], core_in.at[0, lines], ("p1c", d), s, core_mate, "p1c")
         own_sum[...] = project(c)
         for k in z_first:
             own_x(*down(k), True)
+    def wait_core(d):
+        lines = pl.ds(pl.multiple_of((y + d) % Y * tokens, tokens), tokens)
+        arrive(core_in.at[0, lines], ("p1c", d), False)
+
     with scope("wait_p1c"):
-        arrive(core_in.at[0], "p1c")
+        for d in range(1, Y):
+            wait_core(d)
 
     def slot_rows(yy):
         return pl.ds(pl.multiple_of(yy * tokens, tokens), tokens)
@@ -413,6 +460,7 @@
                 there = y_in.at[d - 1, pl.ds(k * part, part)]
                 send(block, there, ("p1y", d, k), s, t_of(yy, c), "after")
     with scope("wait_res"):
+        wait_core(0)
         arrive(res, "res", False)
     q_own = half * 2 + c
     q_mate = other * 2 + c
@@ -439,65 +487,102 @@
             for d in range(1, Y):
                 send(block, block, ("ay", d), s, t_of((y + d) % Y, c), "after")
         block = block_at(y, q_own)
-        send(block, block, "ad", s, core_mate)
+        send(block, block, "ad_own", s, core_mate)
     with scope("bulk_a"):
+        for k in x_first[S3:]:
+            own_z(*down(k), True)
         for k in z_first[:3]:
             forward_x(*down(k))
         for k in x_first[: nx - 1]:
-            own_z(*down(k), True)
             forward_z(*down(k))
 
+    width = hidden.shape[1]
+    spans = [(at, min(512, width - at)) for at in range(0, width, 512)]
+    side_size = 2 * quarter
+    step = min(64, tokens)
+
+    def scaled_rows(side):
+        cols = pl.ds(pl.multiple_of(side * side_size, side_size), side_size)
+        gain = norm_scale[:, cols]
+        for yy in range(2):
+            for at in range(0, tokens, step):
+                stream = full[yy, at : at + step, cols].astype(f32)
+                here = slice(yy * tokens + at, yy * tokens + at + step)
+                squares[side, here] = jnp.sum(stream * stream, axis=1, keepdims=True)
+                normed[side, here] = (stream * gain).astype(bf16)
+
+    def products(side, at, n):
+        rows = pl.ds(pl.multiple_of(side * side_size, side_size), side_size)
+        left = normed[side]
+        return (
+            jnp.dot(left, gate[rows, at : at + n], preferred_element_type=f32),
+            jnp.dot(left, up[rows, at : at + n], preferred_element_type=f32),
+        )
+
+    def early(at, n):
+        gate_part, up_part = products(half, at, n)
+        gate_sum[:, at : at + n] = gate_part
+        up_sum[:, at : at + n] = up_part
+
+    def pass_az(k):
+        block = block_at(y, q_mate, k)
+        arrive(block, ("az", k), False)
+        for d in range(1, Y):
+            send(block, block, ("ayz", d, k), s, t_of((y + d) % Y, c), "after")
+        send(block, block, "ad_mate", s, core_mate)
+
+    def pass_ayz(k):
+        for d in range(1, Y):
+            block = block_at((y - d + Y) % Y, q_mate, k)
+            arrive(block, ("ayz", d, k), False)
+            send(block, block, "ad_mate", s, core_mate)
+
+    with scope("wait_az"):
+        for k in range(PIECES // 2):
+            pass_az(k)
     with scope("wait_ay"):
         for d in range(1, Y):
             block = block_at((y - d + Y) % Y, q_own)
             arrive(block, ("ay", d), False)
-            send(block, block, "ad", s, core_mate)
-    with scope("wait_az"):
-        for k in range(PIECES):
-            block = block_at(y, q_mate, k)
-            arrive(block, ("az", k), False)
-            for d in range(1, Y):
-                send(block, block, ("ayz", d, k), s, t_of((y + d) % Y, c), "after")
-            send(block, block, "ad", s, core_mate)
+            send(block, block, "ad_own", s, core_mate)
+    with scope("wait_az2"):
+        for k in range(PIECES // 2, PIECES):
+            pass_az(k)
     with scope("bulk_b"):
         for k in z_first[3:]:
             forward_x(*down(k))
         for k in x_first[nx - 1 :]:
-            own_z(*down(k), True)
             forward_z(*down(k))
-    with scope("wait_ayz"):
-        for k in range(PIECES):
-            for d in range(1, Y):
-                block = block_at((y - d + Y) % Y, q_mate, k)
-                arrive(block, ("ayz", d, k), False)
-                send(block, block, "ad", s, core_mate)
+    with scope("early"):
+        arrive(full.at[0, :, pl.ds(0, side_size)], "ad_own")
+        for copy in moving[7:9]:
+            copy.wait()
+        moving[10].wait()
+        scaled_rows(half)
+        for i, span in enumerate(spans):
+            early(*span)
+            if i < PIECES:
+                pass_ayz(i)
+        for k in range(len(spans), PIECES):
+            pass_ayz(k)
     with scope("wait_ad"):
-        arrive(full.at[0], "ad")
+        arrive(full.at[0, :, pl.ds(0, side_size)], "ad_mate")
 
     with scope("norm"):
-        step = min(32, tokens)
-        for yy in range(2):
-            for at in range(0, tokens, step):
-                stream = full[yy, at : at + step].astype(f32)
-                scaled = stream * lax.rsqrt(
-                    jnp.mean(stream * stream, axis=1, keepdims=True) + epsilon
-                )
-                normed[yy * tokens + at : yy * tokens + at + step] = (
-                    scaled * norm_gain[...]
-                ).astype(bf16)
-
-    for copy in moving[7:]:
-        copy.wait()
-    width = hidden.shape[1]
-    spans = [(at, min(512, width - at)) for at in range(0, width, 512)]
+        scaled_rows(other)
+        inverse[...] = lax.rsqrt(
+            (squares[0] + squares[1]) * (1.0 / full.shape[2]) + epsilon
+        )
     with scope("gateup"):
-        rows_in = normed[...]
         for at, n in spans:
-            gate_part = jnp.dot(rows_in, gate[:, at : at + n], preferred_element_type=f32)
-            up_part = jnp.dot(rows_in, up[:, at : at + n], preferred_element_type=f32)
+            gate_part, up_part = products(other, at, n)
+            factor = inverse[...]
+            gate_part = (gate_part + gate_sum[:, at : at + n]) * factor
+            up_part = (up_part + up_sum[:, at : at + n]) * factor
             hidden[:, at : at + n] = (
                 gate_part / (1.0 + jnp.exp(-gate_part)) * up_part
             ).astype(bf16)
+
     place = q_own * Y + y
     unit = prod.shape[2]
     half_unit = unit // 2
@@ -513,14 +598,12 @@
         prod[i] = lax.dot_general(hidden[...], weight, ROWS_ROWS, preferred_element_type=f32)
         cols = pl.ds(pl.multiple_of((1 - c) * half_unit, half_unit), half_unit)
         lower_out[i] = prod[i, :, cols].astype(bf16)
-
-    def pass_on(lo, n, name):
+        send(lower_out.at[i], lower_in.at[i], ("p2c", i), s, core_mate, "p2c")
+
+    def to_owners(lo, n, name):
         units = pl.ds(lo, n)
-        send(lower_out.at[units], lower_in.at[units], name, s, core_mate)
-
-    def to_owners(lo, n, name, core_name):
-        units = pl.ds(lo, n)
-        arrive(lower_in.at[units], core_name)
+        for i in range(lo, lo + n):
+            arrive(lower_in.at[i], ("p2c", i), False)
         cols = pl.ds(pl.multiple_of(c * half_unit, half_unit), half_unit)
         for i in range(lo, lo + n):
             total = prod[i, :, cols] + lower_in[i].astype(f32)
@@ -558,16 +641,15 @@
             with scope("wait_z"):
                 wait_z()
         lower(2)
-        pass_on(0, 3, "p2c")
     with scope("owners_a"):
-        to_owners(0, 3, "p2o", "p2c")
+        to_owners(0, 2, "p2o")
+        to_owners(2, 1, "p3o")
     if staged:
         with scope("wait_rest"):
             wait_rest()
     with scope("down_b"):
         lower(3)
-        pass_on(3, 1, "p3c")
-        to_owners(3, 1, "p3o", "p3c")
+        to_owners(3, 1, "p4o")
     mine = pl.ds(pl.multiple_of(t * piece, piece), piece)
 
     def finish(lo, n, name):
@@ -582,9 +664,11 @@
                 result[:, cols] = (full[half, mine, cols].astype(f32) + total).astype(bf16)
 
     with scope("wait_p2o"):
-        finish(0, 3, "p2o")
+        finish(0, 2, "p2o")
     with scope("wait_p3o"):
-        finish(3, 1, "p3o")
+        finish(2, 1, "p3o")
+    with scope("wait_p4o"):
+        finish(3, 1, "p4o")
     with scope("wait_send"):
         for ref, name in sends:
             sent(ref, name)
@@ -592,6 +676,8 @@
         sent(downw.at[pl.ds(0, (G - 1) * down_rows)], "down")
         assert 3 * (Y - 1) + 1 == 4
         sent(full.at[0], "after")
+        sent(core_in.at[0], "p1c")
+        sent(lower_in, "p2c")
         sent(res.at[pl.ds(0, 3)], "res")
 
         @pl.when(y != half)
@@ -623,12 +709,13 @@
     smem = pl.BlockSpec(memory_space=pltpu.SMEM)
     Zh = Z // 2
     z_first = C - X_FIRST if C > X_FIRST else C
-    received = 20 + 4 * PIECES + (OC + z_first) * (Zh - 1) + (C - z_first) * (X - 1)
+    received = 20 + 4 * PIECES + (OC + z_first) * (Zh - 1) + (C - z_first + OC) * (X - 1)
     return pl.pallas_call(
         functools.partial(kernel, Z, X, T, C, OC, heads),
-        out_shape=jax.ShapeDtypeStruct((piece, model), bf16),
+        out_shape=pltpu.VMEM((piece, model), bf16),
         in_specs=[
-            anywhere, anywhere, anywhere, anywhere, anywhere, anywhere, smem, vmem, anywhere, vmem,
+            anywhere, anywhere, anywhere, anywhere, anywhere, anywhere, smem, anywhere, anywhere,
+            anywhere,
             anywhere, anywhere, anywhere,
         ],
         out_specs=vmem,
@@ -644,6 +731,10 @@
             pltpu.VMEM((G * rows_down, width), bf16),
             pltpu.VMEM(gate_weight.shape, bf16),
             pltpu.VMEM(up_weight.shape, bf16),
+            pltpu.VMEM((1, head_gain.shape[0]), jnp.float32),
+            pltpu.VMEM((1, norm_gain.shape[0]), jnp.float32),
+            pltpu.VMEM((heads, 2 * tokens, min(sp * tokens, 1024)), bf16),
+            pltpu.VMEM((heads, 2 * tokens, 1), jnp.float32),
             pltpu.VMEM((heads, tokens, vd), bf16),
             pltpu.VMEM((2, tokens, vw), bf16),
             pltpu.VMEM((T, piece, quarter), bf16),
@@ -656,12 +747,16 @@
             pltpu.VMEM((Y - 1, tokens, quarter), bf16),
             pltpu.VMEM((2 * tokens, quarter), jnp.float32),
             pltpu.VMEM((2, tokens, model), bf16),
-            pltpu.VMEM((2 * tokens, model), bf16),
+            pltpu.VMEM((2, 2 * tokens, model // 2), bf16),
+            pltpu.VMEM((2, 2 * tokens, 1), jnp.float32),
+            pltpu.VMEM((2 * tokens, 1), jnp.float32),
+            pltpu.VMEM((2 * tokens, width), jnp.float32),
+            pltpu.VMEM((2 * tokens, width), jnp.float32),
             pltpu.VMEM((2 * tokens, width), bf16),
             pltpu.VMEM((2, T, 4, piece, model // 16), bf16),
             pltpu.VMEM((4 * Y, 4, piece, model // 16), bf16),
-            pltpu.SemaphoreType.DMA((9,)),
-            pltpu.SemaphoreType.DMA((16,)),
+            pltpu.SemaphoreType.DMA((11,)),
+            pltpu.SemaphoreType.DMA((20,)),
             pltpu.SemaphoreType.DMA((received,)),
         ],
         compiler_params=pltpu.CompilerParams(

time: 64.8 us -> 61.1 us (0.943)
  Pallas kernels: 63 us -> 60.2 us
  local copies, waits for them, and re-layouts: 1.57 us -> 0.66 us
    pallas_call x1, Pallas kernels: 63 us -> 60.2 us  [local(): pl.pallas_call(functools.partial(kernel, Z, X, T, C, OC, heads), out_shap...]
    unnamed x1, local copies, waits for them, and re-layouts: 1.57 us -> 0.66 us
where the time goes in v2:
time: 61.1 us; the launch traced here: 60.9 us
  Pallas kernels  60.2 us (99%)
  local copies, waits for them, and re-layouts  0.66 us (1%)
    pallas_call x1, Pallas kernels, local(): pl.pallas_call(functools.partial(kernel, Z, X, T, C, OC, heads), out_shap...  60.2 us

profile of v2, /device:TPU:0, one launch (start us, length us, event | category | flops | bytes accessed | tf_op | source)
XLA Modules:
  0.0 60.9 jit_solution(2870991914707548776)
XLA Ops:
  0.0 60.2 %shard_map.127 = bf16[32,2048]{1,0:T(8,128)(2,1)S(1)} custom-call(bf16[32,2048]{1,0:T(8,128)(2,1)} %residual.1, bf16[128,256]{1,0:T(8,128)(2,1)} %q_one.1, bf16[128,256]{1,0:T(8,128)(2,1)} %k_one.1, bf16[128,256]{1,0:T(8,128)(2,1)} %q_two.1, bf16[128,256]{1,0:T(8,128)(2,1)} %k_two.1, bf16[128,512]{1,0:T(8,128)(2,1)} %values.1, f32[4]{0:T(128)} %lam.1, ...), custom_call_target="tpu_custom_call" | custom-call | tf_op jit(solution)/shard_map/pallas_call | solution.py:713
  60.3 0.7 %copy.15 = bf16[32,2048]{1,0:T(8,128)(2,1)} copy(bf16[32,2048]{1,0:T(8,128)(2,1)S(1)} %shard_map.127) | data formatting | bytes 262144

commit v3 on v2

--- a/solution.py
+++ b/solution.py
@@ -10,6 +10,7 @@
 epsilon = 1e-06
 ROWS_ROWS = (((1,), (1,)), ((), ()))
 CHUNKS = 8
+S4 = 0
 S3 = 1
 X_FIRST = 3
 OUT_CHUNKS = 4
@@ -61,6 +62,7 @@
     up,
     head_scale,
     norm_scale,
+    weights,
     rounded_all,
     totals_all,
     att_out,
@@ -139,6 +141,7 @@
         (up_weight, up),
         (head_gain, head_scale),
         (norm_gain, norm_scale),
+        (lam, weights),
     ]
     moving = [
         pltpu.make_async_copy(src, dst, local_sem.at[i]) for i, (src, dst) in enumerate(moves)
@@ -238,19 +241,19 @@
             to = group + "_x" if last else (name, "x", d)
             send(ref(zl, x), ref(zl, x), to, x_at(d), t, group)
 
-    def forward_x(name, ref, group):
+    def forward_x(name, ref, group, late=False):
         for d in range(1, Zh):
             block = ref(zl_from(d), x)
             arrive(block, (name, "z", d), False)
             for dx in range(1, X):
-                send(block, block, group + "_rest", x_at(dx), t, group)
-
-    def forward_z(name, ref, group):
+                send(block, block, group + ("_late" if late else "_rest"), x_at(dx), t, group)
+
+    def forward_z(name, ref, group, late=False):
         for d in range(1, X):
             block = ref(zl, x_from(d))
             arrive(block, (name, "x", d), False)
             for dz in range(1, Zh):
-                send(block, block, group + "_rest", z_at(dz), t, group)
+                send(block, block, group + ("_late" if late else "_rest"), z_at(dz), t, group)
 
     def down(k):
         return "down%d" % k, down_part(k), "down"
@@ -346,11 +349,12 @@
         return state[2] / state[1]
 
     moving[9].wait()
+    moving[11].wait()
     head_cols = pl.ds(pl.multiple_of(h * value_size, value_size), value_size)
     turns = (*range(1, heads), 0)
 
     def attend(d, both):
-        difference = both[:tokens] - lam[h] * both[tokens:]
+        difference = both[:tokens] - weights[h] * both[tokens:]
         scaled = difference * lax.rsqrt(
             jnp.mean(difference * difference, axis=1, keepdims=True) + epsilon
         )
@@ -411,6 +415,8 @@
         own_z(*down(k), False)
     for k in x_first[:S3]:
         own_z(*down(k), True)
+    for k in x_first[:S4]:
+        forward_z(*down(k), 2 * k >= C)
     for k in x_first[S0 + S1 :]:
         own_x(*down(k), False)
 
@@ -492,35 +498,38 @@
         for k in x_first[S3:]:
             own_z(*down(k), True)
         for k in z_first[:3]:
-            forward_x(*down(k))
-        for k in x_first[: nx - 1]:
-            forward_z(*down(k))
+            forward_x(*down(k), 2 * k >= C)
+        for k in x_first[S4 : nx - 1]:
+            forward_z(*down(k), 2 * k >= C)
 
     width = hidden.shape[1]
     spans = [(at, min(512, width - at)) for at in range(0, width, 512)]
     side_size = 2 * quarter
     step = min(64, tokens)
 
-    def scaled_rows(side):
-        cols = pl.ds(pl.multiple_of(side * side_size, side_size), side_size)
+    def scaled_rows(side, start, size):
+        cols = pl.ds(pl.multiple_of(side * side_size + start, quarter), size)
+        inner = pl.ds(start if isinstance(start, int) else pl.multiple_of(start, quarter), size)
         gain = norm_scale[:, cols]
         for yy in range(2):
             for at in range(0, tokens, step):
                 stream = full[yy, at : at + step, cols].astype(f32)
                 here = slice(yy * tokens + at, yy * tokens + at + step)
-                squares[side, here] = jnp.sum(stream * stream, axis=1, keepdims=True)
-                normed[side, here] = (stream * gain).astype(bf16)
-
-    def products(side, at, n):
-        rows = pl.ds(pl.multiple_of(side * side_size, side_size), side_size)
-        left = normed[side]
+                part = jnp.sum(stream * stream, axis=1, keepdims=True)
+                squares[here] = part if size == side_size else squares[here] + part
+                normed[side, here, inner] = (stream * gain).astype(bf16)
+
+    def products(side, start, size, at, n):
+        rows = pl.ds(pl.multiple_of(side * side_size + start, quarter), size)
+        inner = pl.ds(start if isinstance(start, int) else pl.multiple_of(start, quarter), size)
+        left = normed[side, :, inner]
         return (
             jnp.dot(left, gate[rows, at : at + n], preferred_element_type=f32),
             jnp.dot(left, up[rows, at : at + n], preferred_element_type=f32),
         )
 
     def early(at, n):
-        gate_part, up_part = products(half, at, n)
+        gate_part, up_part = products(half, 0, side_size, at, n)
         gate_sum[:, at : at + n] = gate_part
         up_sum[:, at : at + n] = up_part
 
@@ -550,32 +559,36 @@
             pass_az(k)
     with scope("bulk_b"):
         for k in z_first[3:]:
-            forward_x(*down(k))
+            forward_x(*down(k), 2 * k >= C)
         for k in x_first[nx - 1 :]:
-            forward_z(*down(k))
+            forward_z(*down(k), 2 * k >= C)
     with scope("early"):
         arrive(full.at[0, :, pl.ds(0, side_size)], "ad_own")
         for copy in moving[7:9]:
             copy.wait()
         moving[10].wait()
-        scaled_rows(half)
+        scaled_rows(half, 0, side_size)
         for i, span in enumerate(spans):
             early(*span)
             if i < PIECES:
                 pass_ayz(i)
         for k in range(len(spans), PIECES):
             pass_ayz(k)
+    with scope("middle"):
+        scaled_rows(other, c * quarter, quarter)
+        for at, n in spans:
+            gate_part, up_part = products(other, c * quarter, quarter, at, n)
+            gate_sum[:, at : at + n] += gate_part
+            up_sum[:, at : at + n] += up_part
     with scope("wait_ad"):
         arrive(full.at[0, :, pl.ds(0, side_size)], "ad_mate")
 
     with scope("norm"):
-        scaled_rows(other)
-        inverse[...] = lax.rsqrt(
-            (squares[0] + squares[1]) * (1.0 / full.shape[2]) + epsilon
-        )
+        scaled_rows(other, (1 - c) * quarter, quarter)
+        inverse[...] = lax.rsqrt(squares[...] * (1.0 / full.shape[2]) + epsilon)
     with scope("gateup"):
         for at, n in spans:
-            gate_part, up_part = products(other, at, n)
+            gate_part, up_part = products(other, (1 - c) * quarter, quarter, at, n)
             factor = inverse[...]
             gate_part = (gate_part + gate_sum[:, at : at + n]) * factor
             up_part = (up_part + up_sum[:, at : at + n]) * factor
@@ -624,13 +637,17 @@
         if x_first:
             arrive(downw.at[pl.ds(0, nx * (Zh - 1) * size)], "down_z", False)
 
-    def wait_rest():
-        arrive(downw.at[pl.ds(0, (X - 1) * (Zh - 1) * down_rows)], "down_rest", False)
+    def wait_rest(late):
+        count = C // 2 if late else C - C // 2
+        if count:
+            rows = pl.ds(0, (X - 1) * (Zh - 1) * count * size)
+            arrive(downw.at[rows], "down_late" if late else "down_rest", False)
 
     if not staged:
         wait_x()
         wait_z()
-        wait_rest()
+        wait_rest(False)
+        wait_rest(True)
     with scope("down_a"):
         lower(0)
         if staged:
@@ -640,15 +657,27 @@
         if staged:
             with scope("wait_z"):
                 wait_z()
+        to_owners(0, 1, "p1o")
         lower(2)
     with scope("owners_a"):
-        to_owners(0, 2, "p2o")
+        to_owners(1, 1, "p2o")
         to_owners(2, 1, "p3o")
-    if staged:
-        with scope("wait_rest"):
-            wait_rest()
-    with scope("down_b"):
-        lower(3)
+    start = order[3] * unit
+    for side in range(2):
+        if staged:
+            with scope("wait_rest"):
+                wait_rest(bool(side))
+        with scope("down_b"):
+            weight = downw[pl.ds(pl.multiple_of(start + side * half_unit, half_unit), half_unit)]
+            product = lax.dot_general(hidden[...], weight, ROWS_ROWS, preferred_element_type=f32)
+            prod[3, :, side * half_unit : (side + 1) * half_unit] = product
+
+            @pl.when(c != side)
+            def _():
+                lower_out[3] = product.astype(bf16)
+                send(lower_out.at[3], lower_in.at[3], ("p2c", 3), s, core_mate, "p2c")
+
+    with scope("owners_b"):
         to_owners(3, 1, "p4o")
     mine = pl.ds(pl.multiple_of(t * piece, piece), piece)
 
@@ -664,7 +693,8 @@
                 result[:, cols] = (full[half, mine, cols].astype(f32) + total).astype(bf16)
 
     with scope("wait_p2o"):
-        finish(0, 2, "p2o")
+        finish(0, 1, "p1o")
+        finish(1, 1, "p2o")
     with scope("wait_p3o"):
         finish(2, 1, "p3o")
     with scope("wait_p4o"):
@@ -706,7 +736,6 @@
     Y = T // 2
     vmem = pl.BlockSpec(memory_space=pltpu.VMEM)
     anywhere = pl.BlockSpec(memory_space=pl.ANY)
-    smem = pl.BlockSpec(memory_space=pltpu.SMEM)
     Zh = Z // 2
     z_first = C - X_FIRST if C > X_FIRST else C
     received = 20 + 4 * PIECES + (OC + z_first) * (Zh - 1) + (C - z_first + OC) * (X - 1)
@@ -714,7 +743,7 @@
         functools.partial(kernel, Z, X, T, C, OC, heads),
         out_shape=pltpu.VMEM((piece, model), bf16),
         in_specs=[
-            anywhere, anywhere, anywhere, anywhere, anywhere, anywhere, smem, anywhere, anywhere,
+            anywhere, anywhere, anywhere, anywhere, anywhere, anywhere, anywhere, anywhere, anywhere,
             anywhere,
             anywhere, anywhere, anywhere,
         ],
@@ -733,6 +762,7 @@
             pltpu.VMEM(up_weight.shape, bf16),
             pltpu.VMEM((1, head_gain.shape[0]), jnp.float32),
             pltpu.VMEM((1, norm_gain.shape[0]), jnp.float32),
+            pltpu.SMEM(lam.shape, jnp.float32),
             pltpu.VMEM((heads, 2 * tokens, min(sp * tokens, 1024)), bf16),
             pltpu.VMEM((heads, 2 * tokens, 1), jnp.float32),
             pltpu.VMEM((heads, tokens, vd), bf16),
@@ -748,15 +778,15 @@
             pltpu.VMEM((2 * tokens, quarter), jnp.float32),
             pltpu.VMEM((2, tokens, model), bf16),
             pltpu.VMEM((2, 2 * tokens, model // 2), bf16),
-            pltpu.VMEM((2, 2 * tokens, 1), jnp.float32),
+            pltpu.VMEM((2 * tokens, 1), jnp.float32),
             pltpu.VMEM((2 * tokens, 1), jnp.float32),
             pltpu.VMEM((2 * tokens, width), jnp.float32),
             pltpu.VMEM((2 * tokens, width), jnp.float32),
             pltpu.VMEM((2 * tokens, width), bf16),
             pltpu.VMEM((2, T, 4, piece, model // 16), bf16),
             pltpu.VMEM((4 * Y, 4, piece, model // 16), bf16),
-            pltpu.SemaphoreType.DMA((11,)),
-            pltpu.SemaphoreType.DMA((20,)),
+            pltpu.SemaphoreType.DMA((12,)),
+            pltpu.SemaphoreType.DMA((21,)),
             pltpu.SemaphoreType.DMA((received,)),
         ],
         compiler_params=pltpu.CompilerParams(

time: 61.1 us -> 60.6 us (level)
  no operation moved by 1% of the time
where the time goes in v3:
time: 60.6 us; the launch traced here: 60.4 us
  Pallas kernels  59.8 us (99%)
  local copies, waits for them, and re-layouts  0.66 us (1%)
    pallas_call x1, Pallas kernels, local(): pl.pallas_call(functools.partial(kernel, Z, X, T, C, OC, heads), out_shap...  59.8 us

profile of v3, /device:TPU:0, one launch (start us, length us, event | category | flops | bytes accessed | tf_op | source)
XLA Modules:
  0.0 60.4 jit_solution(2629225836929361546)
XLA Ops:
  0.0 59.8 %shard_map.127 = bf16[32,2048]{1,0:T(8,128)(2,1)S(1)} custom-call(bf16[32,2048]{1,0:T(8,128)(2,1)} %residual.1, bf16[128,256]{1,0:T(8,128)(2,1)} %q_one.1, bf16[128,256]{1,0:T(8,128)(2,1)} %k_one.1, bf16[128,256]{1,0:T(8,128)(2,1)} %q_two.1, bf16[128,256]{1,0:T(8,128)(2,1)} %k_two.1, bf16[128,512]{1,0:T(8,128)(2,1)} %values.1, f32[4]{0:T(128)} %lam.1, ...), custom_call_target="tpu_custom_call" | custom-call | tf_op jit(solution)/shard_map/pallas_call | solution.py:742
  59.8 0.7 %copy.15 = bf16[32,2048]{1,0:T(8,128)(2,1)} copy(bf16[32,2048]{1,0:T(8,128)(2,1)S(1)} %shard_map.127) | data formatting | bytes 262144

commit v4 on v3

--- a/solution.py
+++ b/solution.py
@@ -18,7 +18,7 @@
 S1 = 1
 S2 = 5
 OUT_X_FIRST = 0
-PIECES = 4
+PIECES = 8
 
 
 def split_sp(size):
@@ -738,7 +738,7 @@
     anywhere = pl.BlockSpec(memory_space=pl.ANY)
     Zh = Z // 2
     z_first = C - X_FIRST if C > X_FIRST else C
-    received = 20 + 4 * PIECES + (OC + z_first) * (Zh - 1) + (C - z_first + OC) * (X - 1)
+    received = 21 + 3 * PIECES + (OC + z_first) * (Zh - 1) + (C - z_first + OC) * (X - 1)
     return pl.pallas_call(
         functools.partial(kernel, Z, X, T, C, OC, heads),
         out_shape=pltpu.VMEM((piece, model), bf16),

time: 60.6 us -> 60.6 us (level)
  no operation moved by 1% of the time
where the time goes in v4:
time: 60.6 us; the launch traced here: 60.5 us
  Pallas kernels  59.8 us (99%)
  local copies, waits for them, and re-layouts  0.66 us (1%)
    pallas_call x1, Pallas kernels, local(): pl.pallas_call(functools.partial(kernel, Z, X, T, C, OC, heads), out_shap...  59.8 us

profile of v4, /device:TPU:0, one launch (start us, length us, event | category | flops | bytes accessed | tf_op | source)
XLA Modules:
  0.0 60.5 jit_solution(13276797891500099124)
XLA Ops:
  0.0 59.8 %shard_map.127 = bf16[32,2048]{1,0:T(8,128)(2,1)S(1)} custom-call(bf16[32,2048]{1,0:T(8,128)(2,1)} %residual.1, bf16[128,256]{1,0:T(8,128)(2,1)} %q_one.1, bf16[128,256]{1,0:T(8,128)(2,1)} %k_one.1, bf16[128,256]{1,0:T(8,128)(2,1)} %q_two.1, bf16[128,256]{1,0:T(8,128)(2,1)} %k_two.1, bf16[128,512]{1,0:T(8,128)(2,1)} %values.1, f32[4]{0:T(128)} %lam.1, ...), custom_call_target="tpu_custom_call" | custom-call | tf_op jit(solution)/shard_map/pallas_call | solution.py:742
  59.8 0.7 %copy.15 = bf16[32,2048]{1,0:T(8,128)(2,1)} copy(bf16[32,2048]{1,0:T(8,128)(2,1)S(1)} %shard_map.127) | data formatting | bytes 262144
